TPU v7x, 512 devices: a whole 4x8x8 slice. The times are simulated.
512 devices in a mesh: ep: 32 (over z, x), tp: 16 (over y, core).
Axes of the slice: x: 4, y: 8, z: 8, core: 2. Of those that a mesh axis runs over, the one named last changes fastest.
Arguments:
- queries: bfloat16 [16384, 1024], P('ep', 'tp'), may hold values from -6 to 6
- key_input: bfloat16 [16384, 256], P('ep'), may hold values from -6 to 6
- value_input: bfloat16 [16384, 256], P('ep'), may hold values from -6 to 6
- query_gain: float32 [64], replicated, may hold values from 0.1 to 1.9
- key_gain: float32 [64], replicated, may hold values from 0.1 to 1.9
- mix_out_weight: bfloat16 [1024, 2048], P('tp'), may hold values from -0.1875 to 0.1875
- expert_input: bfloat16 [5120, 2048], P('ep'), may hold values from -6 to 6
- ffn_gain: float32 [2048], replicated, may hold values from 0.1 to 1.9
- routes: int32 [5120, 2], P('ep'), may hold values from 0 to 31, all different within a row; in each aligned block of 160 rows (0 to 159, 160 to 319, ...) at most 15 rows name the same one
- route_scores: float32 [5120, 2], P('ep'), may hold values from 0.1 to 1
- gate_weight: bfloat16 [32, 2048, 4096], P('ep', None, 'tp'), may hold values from -0.125 to 0.125
- up_weight: bfloat16 [32, 2048, 4096], P('ep', None, 'tp'), may hold values from -0.125 to 0.125
- down_weight: bfloat16 [32, 4096, 2048], P('ep', 'tp'), may hold values from -0.09375 to 0.09375
Outputs:
- mixed_rows: bfloat16 [16384, 2048], P(('ep', 'tp'))
- expert_out: bfloat16 [5120, 2048], P('ep', 'tp')
Inputs may be any that keep to these rules, and one draw needn't show every extreme that they name: `routes`: each row names 2 different experts. Within the rows of one index of ep (aligned blocks of 160 rows) no expert is named by more than 15 rows, and in every draw some expert is named by exactly 15 rows of some block.
All inputs are finite; a program needn't handle non-finite values.
Results may differ from a plain program's by a relative error of at most 0.019.
The roundings to bfloat16 on the way count: a program that leaves them out, or rounds other values in their place, can miss the bound.
Values may be sent and summed in bfloat16 or wider, within the bound.
A program may use at most 64 MiB of HBM per device.

v0:
```python
import math

import jax
import jax.numpy as jnp
from jax import lax
from jax.sharding import PartitionSpec as P

HEADS = 16
KV_HEADS = 4
HD = 64
GRID_W = 64


EPSILON = 1e-06
ROPE_BASE = 10000.0


def in_one_piece(arrays, axis, dim, along):
    both = jnp.concatenate(arrays, axis=along)
    filled, at, finished = (lax.all_gather(both, axis, axis=dim, tiled=True), 0, [])
    for a in arrays:
        finished.append(lax.slice_in_dim(filled, at, at + a.shape[along], axis=along))
        at += a.shape[along]
    return tuple(finished)


def sent_to_all(shard, axis):
    copies = jnp.broadcast_to(shard, (lax.axis_size(axis), *shard.shape))
    return lax.all_to_all(copies, axis, split_axis=0, concat_axis=0, tiled=True)


def laid_out(parts, dim):
    dims = list(parts.shape[1:])
    dims[dim] *= parts.shape[0]
    return jnp.moveaxis(parts, 0, dim).reshape(dims)


def gathered_copies(shard, axis, dim):
    parts = sent_to_all(shard, axis)
    return laid_out(parts, dim)


def rotate_half(portion, cos_table, sin_table):
    front_half, back_half = jnp.split(portion, 2, axis=-1)
    cos_table = cos_table[:, None, :]
    sin_table = sin_table[:, None, :]
    return jnp.concatenate(
        [
            front_half * cos_table - back_half * sin_table,
            back_half * cos_table + front_half * sin_table,
        ],
        axis=-1,
    )


def prepare(source, channel_gain, positions):
    token_count = source.shape[0]
    values_f = source.astype(jnp.float32).reshape(token_count, -1, HD)
    normed = (
        values_f
        * lax.rsqrt(jnp.mean(values_f * values_f, axis=-1, keepdims=True) + EPSILON)
        * channel_gain
    )
    quarter = HD // 4
    inverse = ROPE_BASE ** (-jnp.arange(quarter, dtype=jnp.float32) / quarter)
    row_angle = (positions // GRID_W).astype(jnp.float32)[:, None] * inverse[None, :]
    col_angle = (positions % GRID_W).astype(jnp.float32)[:, None] * inverse[None, :]
    half_width = HD // 2
    turned = jnp.concatenate(
        [
            rotate_half(normed[..., :half_width], jnp.cos(row_angle), jnp.sin(row_angle)),
            rotate_half(normed[..., half_width:], jnp.cos(col_angle), jnp.sin(col_angle)),
        ],
        axis=-1,
    )
    return turned.reshape(token_count, -1).astype(jnp.bfloat16)


def local(
    queries,
    key_input,
    value_input,
    query_gain,
    key_gain,
    mix_out_weight,
    expert_input,
    ffn_gain,
    routes,
    route_scores,
    gate_weight,
    up_weight,
    down_weight,
):
    row_count = queries.shape[0]
    heads_here = queries.shape[1] // HD
    group_size = HEADS // KV_HEADS
    kv_here = max(1, heads_here // group_size)
    sharing = heads_here // kv_here
    tp_count = lax.axis_size("tp")
    tp_index = lax.axis_index("tp")
    positions = lax.axis_index("ep") * row_count + jnp.arange(row_count, dtype=jnp.int32)
    first_kv = tp_index * heads_here // group_size
    own_keys = lax.dynamic_slice_in_dim(key_input, first_kv * HD, kv_here * HD, 1)
    own_values = lax.dynamic_slice_in_dim(value_input, first_kv * HD, kv_here * HD, 1)
    q_rot = prepare(queries, query_gain, positions).reshape(row_count, kv_here, sharing, HD)
    outgoing = prepare(own_keys, key_gain, positions)
    start_state = (
        jnp.zeros((row_count, kv_here, sharing, HD), jnp.float32),
        jnp.zeros((row_count, kv_here, sharing), jnp.float32),
    )
    running = start_state
    key_piece, value_piece = in_one_piece((outgoing, own_values), "ep", 0, 1)
    key_count = key_piece.shape[0]
    key_span = math.gcd(key_count, 1024)
    key_blocks = key_piece.reshape(key_count // key_span, key_span, kv_here, HD)
    value_blocks = value_piece.reshape(key_count // key_span, key_span, kv_here, HD)

    def one_block(partial_value, block_pair):
        key_block, value_block = block_pair
        scores = jnp.einsum(
            "qgrd,kgd->qgrk", q_rot, key_block, preferred_element_type=jnp.float32
        ) * HD ** (-0.5)
        weights = jnp.exp(scores)
        weighted = partial_value[0] + jnp.einsum(
            "qgrk,kgd->qgrd",
            weights.astype(jnp.bfloat16),
            value_block,
            preferred_element_type=jnp.float32,
        )
        return ((weighted, partial_value[1] + jnp.sum(weights, axis=-1)), None)

    running, _ = lax.scan(one_block, running, (key_blocks, value_blocks))
    weighted, denominator = running
    attended = (
        (weighted / denominator[..., None]).astype(jnp.bfloat16).reshape(row_count, heads_here * HD)
    )
    token_count = routes.shape[0]
    top_count = routes.shape[1]
    expert_count = lax.axis_size("ep")
    model_width = expert_input.shape[1]
    feat_width = model_width // tp_count
    capacity = 3 * token_count * top_count // (2 * expert_count)
    flat_routes = routes.reshape(-1)
    hit_table = (flat_routes[:, None] == jnp.arange(expert_count, dtype=jnp.int32)[None, :]).astype(
        jnp.int32
    )
    position = jnp.sum((jnp.cumsum(hit_table, axis=0) - hit_table) * hit_table, axis=1)
    slot_index = flat_routes * capacity + position
    pair_token = jnp.arange(token_count * top_count, dtype=jnp.int32) // top_count
    owner_row = (
        jnp.full((expert_count * capacity,), token_count, jnp.int32).at[slot_index].set(pair_token)
    )
    own_features = lax.dynamic_slice_in_dim(expert_input, tp_index * feat_width, feat_width, 1)
    padded = jnp.concatenate([own_features, jnp.zeros((1, feat_width), jnp.bfloat16)], axis=0)
    outbound = padded[owner_row]
    arrived = lax.all_to_all(outbound, "ep", split_axis=0, concat_axis=0, tiled=True)
    gate_local = gate_weight[0]
    up_local = up_weight[0]
    down_local = down_weight[0]
    values_f = gathered_copies(arrived, "tp", 1).astype(jnp.float32)
    scaled = (values_f * ffn_gain).astype(jnp.bfloat16)
    gate_sum = jnp.dot(scaled, gate_local, preferred_element_type=jnp.float32)
    up_sum = jnp.dot(scaled, up_local, preferred_element_type=jnp.float32)
    squares = jnp.sum(values_f * values_f, axis=1)
    row_scale = lax.rsqrt(squares / model_width + EPSILON)[:, None]
    hidden = (jax.nn.silu(row_scale * gate_sum) * (row_scale * up_sum)).astype(jnp.bfloat16)
    mixed_sum = lax.psum_scatter(
        jnp.dot(attended, mix_out_weight, preferred_element_type=jnp.float32).astype(jnp.bfloat16),
        "tp",
        scatter_dimension=0,
        tiled=True,
    )
    width_sum = lax.psum_scatter(
        lax.dot_general(
            down_local, hidden, (((0,), (1,)), ((), ())), preferred_element_type=jnp.float32
        ).astype(jnp.bfloat16),
        "tp",
        scatter_dimension=0,
        tiled=True,
    )
    returned_rows = lax.all_to_all(width_sum, "ep", split_axis=1, concat_axis=1, tiled=True)
    route_weight = route_scores / jnp.sum(route_scores, axis=-1, keepdims=True)
    picked = returned_rows[:, slot_index].astype(jnp.float32) * route_weight.reshape(-1)[None, :]
    combined = jnp.sum(picked.reshape(feat_width, token_count, top_count), axis=-1)
    return (mixed_sum, combined.T.astype(jnp.bfloat16))


def solution(mesh):
    placed = (
        P("ep", "tp"),
        P("ep", None),
        P("ep", None),
        P(),
        P(),
        P("tp", None),
        P("ep", None),
        P(),
        P("ep", None),
        P("ep", None),
        P("ep", None, "tp"),
        P("ep", None, "tp"),
        P("ep", "tp", None),
    )
    return jax.shard_map(
        local,
        mesh=mesh,
        in_specs=placed,
        out_specs=(P(("ep", "tp"), None), P("ep", "tp")),
        check_vma=False,
    )
```

profile of v0, /device:TPU:1, one launch (start us, length us, event | category | flops | bytes accessed | tf_op | source)
XLA Modules:
  0.0 236.2 jit_solution(2055582904723203697)
XLA Ops:
  15.8 2.9 %scatter_custom_fusion = s32[480]{0:T(512)S(1)} fusion(s32[320]{0:T(512)S(1)} %fusion.99, s32[320]{0:T(512)S(1)} %add_select_fusion, s32[]{:T(128)} %constant.122.clone.1), kind=kCustom, calls=%fused_computation.141 | custom fusion | bytes 1924 | tf_op jit(solution)/shard_map/scatter | solution.py:151
  18.7 1.5 gather_fusion
  20.3 22.8 %all_to_all.29 = bf16[32,15,128]{2,1,0:T(8,128)(2,1)S(1)} all-to-all(bf16[32,15,128]{2,1,0:T(8,128)(2,1)S(1)} %all_to_all.19), channel_id=1, replica_groups=mesh['ep'=32,'tp'=16] {'ep'}, dimensions={0} | all-to-all | bytes 245760 | tf_op jit(solution)/shard_map/all_to_all | solution.py:156
  43.2 1.6 broadcast_in_dim.14
  44.7 10.0 %all-to-all-start.1 = ((bf16[16,480,128]{2,1,0:T(8,128)(2,1)}), bf16[16,480,128]{2,1,0:T(8,128)(2,1)S(1)}, u32[]{:S(2)}, u32[]{:S(2)}) async-start(bf16[16,480,128]{2,1,0:T(8,128)(2,1)} %broadcast_in_dim.14), calls=%async_computation.2 | async-start | bytes 3932160 | tf_op jit(solution)/shard_map/all_to_all | solution.py:29
  54.9 46.3 %all-to-all-done.1 = bf16[16,480,128]{2,1,0:T(8,128)(2,1)S(1)} async-done(((bf16[16,480,128]{2,1,0:T(8,128)(2,1)}), bf16[16,480,128]{2,1,0:T(8,128)(2,1)S(1)}, u32[]{:S(2)}, u32[]{:S(2)}) %all-to-all-start.1) | async-done | bytes 1966112 | tf_op jit(solution)/shard_map/all_to_all | solution.py:29
  103.2 1.5 fusion.26
  104.7 4.1 %fusion.18 = bf16[2048,480]{0,1:T(8,128)(2,1)S(1)} fusion(bf16[16,60,8,128]{3,2,1,0:T(8,128)(2,1)} %copy-done.1, bf16[1,256,2048]{2,1,0:T(8,128)(2,1)S(1)} %copy-done, bf16[1,2048,256]{2,1,0:T(8,128)(2,1)} %param.26, f32[480,256]{1,0:T(8,128)} %fusion.26, f32[480]{0:T(512)S(1)} %add_rsqrt_fusion), kind=kOutput, calls=%fused_computation.27 | convolution fusion | flops 1008476160 | bytes 6522752 | tf_op jit(solution)/shard_map/dot_general | solution.py:174
  108.8 2.5 %copy.36 = bf16[2048,480]{1,0:T(8,128)(2,1)} copy(bf16[2048,480]{0,1:T(8,128)(2,1)S(1)} %fusion.18) | data formatting | bytes 3932160
  111.6 2.6 %fusion.104 = (bf16[16384,64]{0,1:T(8,128)(2,1)S(1)}, bf16[16384,64]{0,1:T(8,128)(2,1)S(1)}) fusion(bf16[16384,128]{0,1:T(8,128)(2,1)} %all-gather.2.cloned.1.call-done), kind=kLoop, calls=%fused_computation.148 | loop fusion | bytes 8388608 | tf_op jit(solution)/shard_map/slice | solution.py:22
  115.4 2.5 %copy.28 = bf16[16,1024,1,64]{1,3,2,0:T(8,128)(2,1)} copy(bf16[16,1024,1,64]{1,0,3,2:T(8,128)(2,1)S(1)} %bitcast.117) | data formatting | bytes 4194304
  119.1 2.4 %copy.29 = bf16[16,1024,1,64]{1,3,2,0:T(8,128)(2,1)} copy(bf16[16,1024,1,64]{1,0,3,2:T(8,128)(2,1)S(1)} %bitcast.118) | data formatting | bytes 4194304
  121.5 45.0 %while.13 = (s32[]{:T(128)}, f32[512,1,1,64]{0,3,2,1:T(8,128)S(1)}, f32[512,1,1]{0,2,1:T(1,128)S(1)}, bf16[16,1024,1,64]{1,3,2,0:T(8,128)(2,1)}, bf16[16,1024,1,...) while((s32[]{:T(128)}, f32[512,1,1,64]{0,3,2,1:T(8,128)S(1)}, ...), condition=%wide.region_4.5_spmd.clone, body=%wide.region_2.4_spmd.clone.sunk | while | flops 136380928 | bytes 4793440 | solution.py:132
  121.5 1.4 fusion.113
  124.3 1.4 fusion.113
  127.2 1.4 fusion.113
  130.0 1.4 fusion.113
  132.8 1.4 fusion.113
  135.6 1.4 fusion.113
  138.4 1.4 fusion.113
  141.2 1.4 fusion.113
  144.0 1.4 fusion.113
  146.9 1.4 fusion.113
  149.7 1.4 fusion.113
  155.3 1.4 fusion.113
  160.9 1.4 fusion.113
  163.7 1.4 fusion.113
  166.5 3.0 %convolution_convert_fusion = bf16[512,2048]{1,0:T(8,128)(2,1)} fusion(bf16[64,2048]{1,0:T(8,128)(2,1)} %param.20, f32[512,1,1,64]{0,3,2,1:T(8,128)S(1)} %get-tuple-element.35, f32[512]{0:T(512)S(1)} %bitcast.123), kind=kOutput, calls=%fused_computation.25 | convolution fusion | flops 135331840 | bytes 2492416 | tf_op jit(solution)/shard_map/dot_general | solution.py:168
  171.4 3.9 %all-to-all-start.2 = ((bf16[128,32,15]{0,2,1:T(8,128)(2,1)}), bf16[128,32,15]{0,2,1:T(8,128)(2,1)S(1)}, u32[]{:S(2)}, u32[]{:S(2)}) async-start(bf16[128,32,15]{0,2,1:T(8,128)(2,1)} %all_to_all.23), calls=%async_computation.3 | async-start | bytes 262144 | tf_op jit(solution)/shard_map/all_to_all | solution.py:181
  175.4 9.3 %all-to-all-done.2 = bf16[128,32,15]{0,2,1:T(8,128)(2,1)S(1)} async-done(((bf16[128,32,15]{0,2,1:T(8,128)(2,1)}), bf16[128,32,15]{0,2,1:T(8,128)(2,1)S(1)}, u32[]{:S(2)}, u32[]{:S(2)}) %all-to-all-start.2) | async-done | bytes 122912 | tf_op jit(solution)/shard_map/all_to_all | solution.py:181
  184.8 1.4 gather_fusion.1
  187.1 41.6 %reduce-scatter.5.cloned.1.call-done = bf16[32,2048]{1,0:T(8,128)(2,1)} async-done(((bf16[512,2048]{1,0:T(8,128)(2,1)}), bf16[32,2048]{1,0:T(8,128)(2,1)}) %reduce-scatter.5.cloned.1.call-update) | async-done | bytes 131088 | tf_op jit(solution)/shard_map/reduce_scatter | solution.py:167
  (104 shorter events, 40.3 us)
Async XLA Ops:
  8.0 96.7 %copy-start = (bf16[1,256,2048]{2,1,0:T(8,128)(2,1)S(1)}, bf16[1,256,2048]{2,1,0:T(8,128)(2,1)}, u32[]{:S(2)}) copy-start(bf16[1,256,2048]{2,1,0:T(8,128)(2,1)} %param.27) | copy-start | bytes 3145732
  8.0 5.1 %copy-start.4 = (s32[160,2]{0,1:T(2,128)S(1)}, s32[160,2]{0,1:T(2,128)}, u32[]{:S(2)}) copy-start(s32[160,2]{0,1:T(2,128)} %param.23) | copy-start | bytes 3844
  8.0 103.5 %all-gather.2.cloned.1.call-start = ((), (), s32[]{:S(2)}) async-start(), calls=%async_computation.5 | async-start | bytes 4325376 | tf_op jit(solution)/shard_map/all_gather | solution.py:20
  44.7 56.5 %copy-start.2 = (f32[2048]{0:T(1024)S(1)}, f32[2048]{0:T(1024)}, u32[]{:S(2)}) copy-start(f32[2048]{0:T(1024)} %param.22) | copy-start | bytes 24580
  44.7 56.5 %all-to-all-start.1 = ((bf16[16,480,128]{2,1,0:T(8,128)(2,1)}), bf16[16,480,128]{2,1,0:T(8,128)(2,1)S(1)}, u32[]{:S(2)}, u32[]{:S(2)}) async-start(bf16[16,480,128]{2,1,0:T(8,128)(2,1)} %broadcast_in_dim.14), calls=%async_computation.2 | async-start | bytes 3932160 | tf_op jit(solution)/shard_map/all_to_all | solution.py:29
  54.8 114.9 %reduce-scatter.7.cloned.1.call-start = ((), (), s32[]{:S(2)}) async-start(), calls=%async_computation.7 | async-start | bytes 2228224
  101.2 2.0 copy-start.5
  101.9 1.3 copy-start.1
  111.3 117.4 %reduce-scatter.5.cloned.1.call-start = ((), (), s32[]{:S(2)}) async-start(), calls=%async_computation.6 | async-start | bytes 2228224 | tf_op jit(solution)/shard_map/reduce_scatter | solution.py:167
  166.5 3.1 %copy-start.3 = (f32[160,2]{0,1:T(2,128)S(1)}, f32[160,2]{0,1:T(2,128)}, u32[]{:S(2)}) copy-start(f32[160,2]{0,1:T(2,128)} %param.24) | copy-start | bytes 3844
  171.4 13.3 %all-to-all-start.2 = ((bf16[128,32,15]{0,2,1:T(8,128)(2,1)}), bf16[128,32,15]{0,2,1:T(8,128)(2,1)S(1)}, u32[]{:S(2)}, u32[]{:S(2)}) async-start(bf16[128,32,15]{0,2,1:T(8,128)(2,1)} %all_to_all.23), calls=%async_computation.3 | async-start | bytes 262144 | tf_op jit(solution)/shard_map/all_to_all | solution.py:181
Sparse Core Ops, SparseCore 0:
  13.2 92.6 all-gather.1
Sparse Core Ops, SparseCore 1:
  111.4 52.5 reduce-scatter.6
  169.7 59.0 reduce-scatter.4
where the time goes:
time: 238 us; the launch traced here: 236 us
  waiting for transfers between devices  97.3 us (41%)
  matrix products  52.9 us (22%)
  local copies, waits for them, and re-layouts  26 us (11%)
  blocking collectives  22.8 us (10%)
  between operations  15.8 us (7%)
  starting transfers between devices  14.2 us (6%)
  other arithmetic  6.59 us (3%)
    all_to_all x1, waiting for transfers between devices, sent_to_all(): return lax.all_to_all(copies, axis, split_axis=0, concat_axis=0, tiled=True)  46.3 us
    reduce_scatter x1, waiting for transfers between devices, local(): lax.psum_scatter(jnp.dot(attended, mix_out_weight, preferred_element_type...  41.6 us
    all_to_all x1, blocking collectives, local(): lax.all_to_all(outbound, 'ep', split_axis=0, concat_axis=0, tiled=True)  22.8 us
    dot_general x16, matrix products, one_block(): jnp.einsum('qgrd,kgd->qgrk', q_rot, key_block, preferred_element_type=jnp...  22.3 us
    dot_general x16, matrix products, one_block(): jnp.einsum('qgrk,kgd->qgrd', weights.astype(jnp.bfloat16), value_block, p...  22 us
    unnamed x21, local copies, waits for them, and re-layouts  12.5 us
    all_to_all x1, starting transfers between devices, sent_to_all(): return lax.all_to_all(copies, axis, split_axis=0, concat_axis=0, tiled=True)  10 us
    all_to_all x1, waiting for transfers between devices, local(): lax.all_to_all(width_sum, 'ep', split_axis=1, concat_axis=1, tiled=True)  9.3 us
  transfers between devices with their start and end apart: 5, of which 3 were waited for; matrix products, arithmetic and copies ran while one was open for 33% of the time, Pallas kernels for 0%

commit v1 on v0

v1 whole, which is shorter than its diff:
```python
import functools
import math
from types import SimpleNamespace

import jax
import jax.numpy as jnp
import numpy as np
from jax import lax
from jax.experimental import pallas as pl
from jax.experimental.pallas import tpu as pltpu
from jax.sharding import PartitionSpec as P

HD = 64
GRID_W = 64
EPSILON = 1e-06
ROPE_BASE = 10000.0
SLOTS = 16
MESH = pl.DeviceIdType.MESH
F32 = jnp.float32
BF16 = jnp.bfloat16


def angle_tables(rows):
    quarter = HD // 4
    inverse = (ROPE_BASE ** (-np.arange(quarter, dtype=np.float32) / quarter)).astype(np.float32)
    lane = np.arange(2 * HD)
    freq = inverse[lane % quarter]
    is_row = (lane % HD) < HD // 2
    sign = np.where((lane // quarter) % 2 == 0, -1.0, 1.0).astype(np.float32)

    def table(count, keep):
        angle = (np.arange(count, dtype=np.float32)[:, None] * freq[None, :]).astype(np.float32)
        cos = np.where(keep, np.cos(angle), 0.0).astype(np.float32)
        sin = np.where(keep, np.sin(angle) * sign, 0.0).astype(np.float32)
        return cos, sin

    return table(rows, is_row) + table(GRID_W, ~is_row)


def kernel(
    g,
    kqv,
    key_gain,
    query_gain,
    row_cos,
    row_sin,
    col_cos,
    col_sin,
    tokens,
    routes,
    scores,
    ffn_gain,
    mix_w,
    gate_w,
    up_w,
    down_w,
    mixed_out,
    expert_out,
    kv,
    q_own,
    q_all,
    o_acc,
    o_in,
    att_out,
    att_in,
    att_row,
    w_all,
    tok_own,
    outbound,
    slots,
    wg,
    wu,
    wd,
    gate_acc,
    up_acc,
    sq_acc,
    hidden,
    ring_out,
    ring_in,
    rows_out,
    rows_in,
    hot,
    sem_local,
    sem_kv_s,
    sem_kv_r,
    sem_kvf_s,
    sem_kvf_r,
    sem_q_s,
    sem_q_r,
    sem_o_s,
    sem_o_r,
    sem_a_s,
    sem_a_r,
    sem_w_s,
    sem_w_r,
    sem_wf_s,
    sem_wf_r,
    sem_ex_s,
    sem_ex_r,
    sem_d_s,
    sem_d_r,
    sem_b_s,
    sem_b_r,
    sem_c_s,
    sem_c_r,
    sem_r_s,
    sem_r_r,
):
    nz, nx, ny, ep, tp = g.nz, g.nx, g.ny, g.nz * g.nx, g.ny * 2
    half_ep = ep // 2
    me_e, me_t = lax.axis_index("ep"), lax.axis_index("tp")
    z, x = me_e // nx, me_e % nx
    y, c = me_t // 2, me_t % 2
    sib = me_t + 1 - 2 * c
    own_half = me_e // half_ep
    tq, tok, d, ff = g.tq, g.tok, g.d, g.ff
    feat = d // 4
    par = y % 2

    def send(src, dst, ssem, rsem, to_e, to_t):
        return pltpu.make_async_remote_copy(
            src_ref=src, dst_ref=dst, send_sem=ssem, recv_sem=rsem,
            device_id=(to_e, to_t), device_id_type=MESH,
        )

    def arrived(dst, rsem):
        send(dst, dst, rsem, rsem, me_e, sib).wait_recv()

    def left(src, ssem):
        send(src, src, ssem, ssem, me_e, sib).wait_send()

    def al(v, m):
        return pl.multiple_of(v, m)

    barrier = pltpu.get_barrier_semaphore()

    def greet_plane(i, _):
        pl.semaphore_signal(barrier, inc=1, device_id=((me_e + i) % ep, me_t), device_id_type=MESH)
        pl.semaphore_signal(barrier, inc=1, device_id=((me_e + i) % ep, sib), device_id_type=MESH)
        return 0

    def greet_line(i, _):
        pl.semaphore_signal(barrier, inc=1, device_id=(me_e, (me_t + i) % tp), device_id_type=MESH)
        return 0

    lax.fori_loop(1, ep, greet_plane, 0)
    lax.fori_loop(1, tp, greet_line, 0)

    feat_at = al((par * 2 + c) * feat, feat)
    loads = [
        pltpu.make_async_copy(tokens.at[:, pl.ds(feat_at, feat)], tok_own, sem_local.at[0]),
        pltpu.make_async_copy(mix_w, w_all.at[pl.ds(al(me_t * HD, HD), HD)], sem_local.at[1]),
        pltpu.make_async_copy(gate_w.at[0], wg.at[c], sem_local.at[2]),
        pltpu.make_async_copy(up_w.at[0], wu.at[c], sem_local.at[3]),
        pltpu.make_async_copy(down_w.at[0], wd.at[pl.ds(al(c * ff, ff), ff)], sem_local.at[4]),
    ]
    for copy in loads:
        copy.start()

    r0, r1 = routes[:, 0:1], routes[:, 1:2]
    lanes_e = lax.broadcasted_iota(jnp.int32, (tok, ep), 1)
    hit0 = (lanes_e == r0).astype(F32)
    hit1 = (lanes_e == r1).astype(F32)
    before = (
        lax.broadcasted_iota(jnp.int32, (tok, tok), 1) < lax.broadcasted_iota(jnp.int32, (tok, tok), 0)
    ).astype(BF16)
    count = jnp.dot(before, (hit0 + hit1).astype(BF16), preferred_element_type=F32)
    pos0 = jnp.sum(count * hit0, axis=1, keepdims=True).astype(jnp.int32)
    pos1 = jnp.sum(count * hit1, axis=1, keepdims=True).astype(jnp.int32)
    lanes_s = lax.broadcasted_iota(jnp.int32, (tok, ep * SLOTS), 1)
    hot[0] = (lanes_s == r0 * SLOTS + pos0).astype(BF16)
    hot[1] = (lanes_s == r1 * SLOTS + pos1).astype(BF16)
    loads[0].wait()
    outbound[...] = lax.dot_general(
        hot[0] + hot[1], tok_own[...], (((0,), (0,)), ((), ())), preferred_element_type=F32
    ).astype(BF16)

    lane = lax.broadcasted_iota(jnp.int32, (GRID_W, 2 * HD), 1)
    low = lane < HD
    is_u = (lane // (HD // 4)) % 2 == 0
    gain = jnp.concatenate([key_gain[...], query_gain[...]], axis=1)
    blocks = tq // GRID_W
    row_at = me_e * blocks
    for b in range(blocks):
        at = b * GRID_W
        v = kqv[at : at + GRID_W, 0 : 2 * HD].astype(F32)
        sq = v * v
        s_low = jnp.sum(jnp.where(low, sq, 0.0), axis=1, keepdims=True)
        s_high = jnp.sum(jnp.where(low, 0.0, sq), axis=1, keepdims=True)
        scale = jnp.where(low, lax.rsqrt(s_low * (1.0 / HD) + EPSILON), lax.rsqrt(s_high * (1.0 / HD) + EPSILON))
        n = v * scale * gain
        cos = col_cos[...] + row_cos[pl.ds(row_at + b, 1), :]
        sin = col_sin[...] + row_sin[pl.ds(row_at + b, 1), :]
        swapped = jnp.where(is_u, pltpu.roll(n, 2 * HD - HD // 4, 1), pltpu.roll(n, HD // 4, 1))
        turned = n * cos + swapped * sin
        kv[z, at : at + GRID_W, :] = jnp.where(
            low, turned, kqv[at : at + GRID_W, 2 * HD : 4 * HD].astype(F32)
        ).astype(BF16)
        att_row[at : at + GRID_W, :] = turned
    q_own[...] = jnp.transpose(att_row[...])[HD : 2 * HD, :].astype(BF16)

    pl.semaphore_wait(barrier, 2 * (ep - 1) + tp - 1)

    slot_at = al((me_e % half_ep) * SLOTS, SLOTS)
    to_core = y * 2 + own_half

    def dispatch(i, start):
        to_e = (me_e + i) % ep
        return send(
            outbound.at[pl.ds(al(to_e * SLOTS, SLOTS), SLOTS)],
            slots.at[pl.ds(slot_at, SLOTS), pl.ds(feat_at, feat)],
            sem_d_s.at[i], sem_d_r.at[(me_e % half_ep) * 2 + c], to_e, to_core,
        )

    dispatch_self = pltpu.make_async_copy(
        outbound.at[pl.ds(al(me_e * SLOTS, SLOTS), SLOTS)],
        slots.at[pl.ds(slot_at, SLOTS), pl.ds(feat_at, feat)],
        sem_d_r.at[(me_e % half_ep) * 2 + c],
    )

    def dispatch_start(i, _):
        dispatch(i, True).start()
        return 0

    lax.fori_loop(1, ep, dispatch_start, 0)

    @pl.when(c == own_half)
    def _():
        dispatch_self.start()

    @pl.when(c != own_half)
    def _():
        dispatch(0, True).start()

    def q_copy(i):
        return send(q_own, q_all.at[x], sem_q_s.at[i], sem_q_r.at[x], z * nx + (x + i) % nx, me_t)

    q_self = pltpu.make_async_copy(q_own, q_all.at[x], sem_q_r.at[x])
    q_self.start()
    for i in range(1, nx):
        q_copy(i).start()

    hq = tq // 2
    kv_mine = pl.ds(al(c * hq, hq), hq)
    kv_other = pl.ds(al((1 - c) * hq, hq), hq)

    def kv_copy(i):
        return send(
            kv.at[z, kv_mine], kv.at[z, kv_mine], sem_kv_s.at[i], sem_kv_r.at[z], ((z + i) % nz) * nx + x, me_t
        )

    order = sorted(range(1, nz), key=lambda i: (min(i, nz - i), i))
    for i in order:
        kv_copy(i).start()

    for copy in loads[1:]:
        copy.wait()

    extra = [
        send(wg.at[c], wg.at[c], sem_ex_s.at[0], sem_ex_r.at[0], me_e, sib),
        send(wu.at[c], wu.at[c], sem_ex_s.at[1], sem_ex_r.at[1], me_e, sib),
        send(
            wd.at[pl.ds(al(c * ff, ff), ff)], wd.at[pl.ds(al(c * ff, ff), ff)],
            sem_ex_s.at[2], sem_ex_r.at[2], me_e, sib,
        ),
    ]
    for copy in extra:
        copy.start()

    half_y = ny // 2
    right = ((y + 1) % ny) * 2 + c
    leftward = ((y + ny - 1) % ny) * 2 + c

    def w_block(yy, core):
        return w_all.at[pl.ds(al((yy * 2 + core) * HD, HD), HD)]

    def w_right(s):
        b = w_block((y + ny - s) % ny, c)
        return send(b, b, sem_w_s.at[0, s], sem_w_r.at[0, s], me_e, right)

    def w_left(s):
        b = w_block((y + s) % ny, c)
        return send(b, b, sem_w_s.at[1, s], sem_w_r.at[1, s], me_e, leftward)

    def w_twin(yy):
        b = w_block(yy, c)
        return send(b, b, sem_wf_s.at[yy], sem_wf_r.at[yy], me_e, sib)

    def w_step(s):
        if s > 0:
            from_left = (y + ny - s) % ny
            arrived(w_block(from_left, c), sem_w_r.at[0, s - 1])
            w_twin(from_left).start()
            if s < half_y:
                from_right = (y + s) % ny
                arrived(w_block(from_right, c), sem_w_r.at[1, s - 1])
                w_twin(from_right).start()
        else:
            w_twin(y).start()
        if s < half_y:
            w_right(s).start()
        if s < half_y - 1:
            w_left(s).start()

    score_scale = HD ** (-0.5) * math.log2(math.e)
    kt = min(256, tq)

    def kv_ready(i):
        if i == 0:
            return
        zz = (z + nz - i) % nz
        arrived(kv.at[zz, kv_mine], sem_kv_r.at[zz])
        send(kv.at[zz, kv_mine], kv.at[zz, kv_mine], sem_kvf_s.at[zz], sem_kvf_r.at[zz], me_e, sib).start()

    def attend(i):
        zz = (z + nz - i) % nz
        if i:
            arrived(kv.at[zz, kv_other], sem_kvf_r.at[zz])
        rows = lax.broadcasted_iota(jnp.int32, (80, tq), 0)
        vt = jnp.where(rows < 16, 1.0, jnp.transpose(kv[zz].astype(F32))[48:128, :]).astype(BF16)

        def one(xx, _):
            total = None
            for k in range(tq // kt):
                s_t = jnp.dot(kv[zz, k * kt : (k + 1) * kt, 0:HD], q_all[xx], preferred_element_type=F32)
                p = jnp.exp2(s_t * score_scale).astype(BF16)
                part = jnp.dot(vt[:, k * kt : (k + 1) * kt], p, preferred_element_type=F32)
                total = part if total is None else total + part
            if i:
                o_acc[xx] = o_acc[xx] + total
            else:
                o_acc[xx] = total
            return 0

        lax.fori_loop(0, nx, one, 0)

    def q_ready():
        def one(i, _):
            arrived(q_all.at[i], sem_q_r.at[i])
            return 0

        lax.fori_loop(0, nx, one, 0)

    own_at, other_at = par * (d // 2), (1 - par) * (d // 2)

    def swap(k):
        at = al(own_at + k * feat, feat)
        b = slots.at[:, pl.ds(at, feat)]
        return send(b, b, sem_b_s.at[k], sem_b_r.at[k], me_e, leftward if k == 0 else right)

    def slots_ready():
        for core in range(2):
            at = al(own_at + core * feat, feat)

            def one(j, _):
                arrived(
                    slots.at[pl.ds(al(j * SLOTS, SLOTS), SLOTS), pl.ds(at, feat)], sem_d_r.at[j * 2 + core]
                )
                return 0

            lax.fori_loop(0, half_ep, one, 0)
            swap(core).start()

    def half_products(start, first):
        for k in range(2):
            at = al(start + k * feat, feat)
            v = slots[:, pl.ds(at, feat)].astype(F32)
            sq = jnp.sum(v * v, axis=1, keepdims=True)
            scaled = (v * ffn_gain[:, pl.ds(at, feat)]).astype(BF16)
            for core in range(2):
                gp = jnp.dot(scaled, wg[core, pl.ds(at, feat), :], preferred_element_type=F32)
                up = jnp.dot(scaled, wu[core, pl.ds(at, feat), :], preferred_element_type=F32)
                if first and k == 0:
                    gate_acc[core], up_acc[core] = gp, up
                else:
                    gate_acc[core], up_acc[core] = gate_acc[core] + gp, up_acc[core] + up
            if first and k == 0:
                sq_acc[...] = jnp.broadcast_to(sq, sq_acc.shape)
            else:
                sq_acc[...] = sq_acc[...] + sq

    def ffn_first():
        for k in range(2):
            arrived(wg.at[1 - c], sem_ex_r.at[0]) if k == 0 else arrived(wu.at[1 - c], sem_ex_r.at[1])
        arrived(wd.at[pl.ds(al((1 - c) * ff, ff), ff)], sem_ex_r.at[2])
        half_products(own_at, True)

    def ffn_second():
        for k in range(2):
            arrived(slots.at[:, pl.ds(al(other_at + k * feat, feat), feat)], sem_b_r.at[k])
        half_products(other_at, False)
        scale = lax.rsqrt(sq_acc[:, 0:1] * (1.0 / d) + EPSILON)
        for core in range(2):
            gate = scale * gate_acc[core]
            hidden[:, core * ff : (core + 1) * ff] = (
                gate / (1.0 + jnp.exp(-gate)) * (scale * up_acc[core])
            ).astype(BF16)

    yb = d // ny
    n_slots = half_ep * SLOTS
    hs = n_slots // 2

    def partial_of(dest):
        return jnp.dot(hidden[...], wd[:, pl.ds(al(dest * yb, yb), yb)], preferred_element_type=F32)

    def ring_copy(way, s):
        rows = pl.ds(0, hs if s == 0 else n_slots)
        return send(
            ring_out.at[way, s, rows], ring_in.at[way, s, rows], sem_c_s.at[way, s], sem_c_r.at[way, s],
            me_e, right if way == 0 else leftward,
        )

    def ring_ready(way, s):
        arrived(ring_in.at[way, s, pl.ds(0, hs if s == 0 else n_slots)], sem_c_r.at[way, s])

    def ring_step(s):
        if s == 0:
            block = partial_of((y + half_y) % ny)
            ring_out[0, 0, 0:hs] = block[0:hs].astype(BF16)
            ring_copy(0, 0).start()
            ring_out[1, 0, 0:hs] = block[hs:].astype(BF16)
            ring_copy(1, 0).start()
            return
        for way in range(2):
            dest = (y + half_y - s) % ny if way == 0 else (y + ny - half_y + s) % ny
            block = partial_of(dest)
            ring_ready(way, s - 1)
            if s == 1:
                mine = pl.ds(0, hs) if way == 0 else pl.ds(hs, hs)
                lo, hi = block[0:hs], block[hs:]
                if way == 0:
                    lo = lo + ring_in[0, 0, 0:hs].astype(F32)
                else:
                    hi = hi + ring_in[1, 0, 0:hs].astype(F32)
                ring_out[way, s, 0:hs] = lo.astype(BF16)
                ring_out[way, s, hs:] = hi.astype(BF16)
            else:
                ring_out[way, s] = (block + ring_in[way, s - 1].astype(F32)).astype(BF16)
            ring_copy(way, s).start()

    def back_copy(j, core):
        src_e = c * half_ep + j
        return send(
            rows_out.at[core, pl.ds(al(j * SLOTS, SLOTS), SLOTS)],
            rows_in.at[pl.ds(al(me_e * SLOTS, SLOTS), SLOTS)],
            sem_r_s.at[j, core], sem_r_r.at[me_e], src_e, y * 2 + core,
        )

    def back_self(j, core):
        return pltpu.make_async_copy(
            rows_out.at[core, pl.ds(al(j * SLOTS, SLOTS), SLOTS)],
            rows_in.at[pl.ds(al(me_e * SLOTS, SLOTS), SLOTS)],
            sem_r_r.at[me_e],
        )

    def ring_end():
        s = half_y - 1
        block = partial_of(y)
        for way in range(2):
            ring_ready(way, s)
        if s == 0:
            lo = block[0:hs] + ring_in[0, 0, 0:hs].astype(F32)
            hi = block[hs:] + ring_in[1, 0, 0:hs].astype(F32)
            block = jnp.concatenate([lo, hi], axis=0)
        else:
            block = block + ring_in[0, s].astype(F32) + ring_in[1, s].astype(F32)
        block = block.astype(BF16)
        for core in range(2):
            rows_out[core] = block[:, core * (yb // 2) : (core + 1) * (yb // 2)]

        def one(j, _):
            for core in range(2):
                here = (c * half_ep + j == me_e) & (c == core)

                @pl.when(here)
                def _():
                    back_self(j, core).start()

                @pl.when(jnp.logical_not(here))
                def _():
                    back_copy(j, core).start()

            return 0

        lax.fori_loop(0, half_ep, one, 0)

    def combine():
        def one(j, _):
            arrived(rows_in.at[pl.ds(al(j * SLOTS, SLOTS), SLOTS)], sem_r_r.at[j])
            return 0

        lax.fori_loop(0, ep, one, 0)
        s0, s1 = scores[:, 0:1], scores[:, 1:2]
        whole = s0 + s1
        p0 = jnp.dot(hot[0], rows_in[...], preferred_element_type=F32)
        p1 = jnp.dot(hot[1], rows_in[...], preferred_element_type=F32)
        expert_out[...] = (p0 * (s0 / whole) + p1 * (s1 / whole)).astype(BF16)

    def o_copy(i):
        to_x = (x + i) % nx
        return send(
            o_acc.at[to_x, pl.ds(8, 72)], o_in.at[x], sem_o_s.at[i], sem_o_r.at[x], z * nx + to_x, me_t
        )

    def o_send():
        for i in range(1, nx):
            o_copy(i).start()

    rows_t = tq // tp
    ht = rows_t // 2

    def a_copy(i):
        to_t = (me_t + i) % tp
        return send(
            att_out.at[pl.ds(al(to_t * ht, ht), ht)], att_in.at[pl.ds(al(me_t * ht, ht), ht)],
            sem_a_s.at[i], sem_a_r.at[me_t], me_e, to_t,
        )

    a_self = pltpu.make_async_copy(
        att_out.at[pl.ds(al(me_t * ht, ht), ht)], att_in.at[pl.ds(al(me_t * ht, ht), ht)], sem_a_r.at[me_t]
    )

    def attend_end():
        total = o_acc[x][8:80]
        for i in range(1, nx):
            xx = (x + i) % nx
            arrived(o_in.at[xx], sem_o_r.at[xx])
            total = total + o_in[xx]
        att_t = total[8:72] / total[0:1]
        att = jnp.transpose(jnp.concatenate([att_t, att_t], axis=0))[:, 0:HD]
        for t in range(tp):
            at = t * rows_t
            att_out[t * ht : (t + 1) * ht, :] = jnp.concatenate(
                [att[at : at + ht], att[at + ht : at + rows_t]], axis=1
            ).astype(BF16)
        a_self.start()

        def one(i, _):
            a_copy(i).start()
            return 0

        lax.fori_loop(1, tp, one, 0)

    def project():
        def one(j, _):
            arrived(att_in.at[pl.ds(al(j * ht, ht), ht)], sem_a_r.at[j])
            return 0

        lax.fori_loop(0, tp, one, 0)

        def two(yy, _):
            arrived(w_block(yy, 1 - c), sem_wf_r.at[yy])
            return 0

        lax.fori_loop(0, ny, two, 0)
        pieces = []
        for j in range(tp // 2):
            a = att_in[2 * j * ht : (2 * j + 1) * ht, :]
            b = att_in[(2 * j + 1) * ht : (2 * j + 2) * ht, :]
            top = jnp.concatenate([a[:, 0:HD], b[:, 0:HD]], axis=1)
            low_rows = jnp.concatenate([a[:, HD:], b[:, HD:]], axis=1)
            pieces.append(jnp.concatenate([top, low_rows], axis=0))
        lhs = jnp.concatenate(pieces, axis=1)
        mixed_out[...] = jnp.dot(lhs, w_all[...], preferred_element_type=F32).astype(BF16)

    w_step(0)
    q_ready()
    attend(0)
    work = order
    after = {}
    plan = g.plan(half_y, len(work))
    actions = dict(
        slots=slots_ready, ffn1=ffn_first, ffn2=ffn_second, ring_end=ring_end, o_send=o_send,
        attend_end=attend_end, project=project, combine=combine,
    )
    for name, arg in plan:
        if name == "kv":
            kv_ready(work[arg])
        elif name == "attend":
            attend(work[arg])
        elif name == "w":
            w_step(arg)
        elif name == "ring":
            ring_step(arg)
        else:
            actions[name]()

    def sent_dispatch(i, _):
        left(outbound.at[pl.ds(0, SLOTS)], sem_d_s.at[i])
        return 0

    lax.fori_loop(1, ep, sent_dispatch, 0)

    @pl.when(c != own_half)
    def _():
        left(outbound.at[pl.ds(0, SLOTS)], sem_d_s.at[0])

    for i in range(1, nx):
        q_copy(i).wait_send()
        o_copy(i).wait_send()
    for i in order:
        kv_copy(i).wait_send()
        zz = (z + nz - i) % nz
        left(kv.at[zz, kv_mine], sem_kvf_s.at[zz])
    for copy in extra:
        copy.wait_send()
    for s in range(half_y):
        w_right(s).wait_send()
        if s < half_y - 1:
            w_left(s).wait_send()
        for way in range(2):
            ring_copy(way, s).wait_send()
    for k in range(2):
        swap(k).wait_send()

    def sent_w(yy, _):
        left(w_block(yy, c), sem_wf_s.at[yy])
        return 0

    lax.fori_loop(0, ny, sent_w, 0)

    def sent_back(j, _):
        for core in range(2):
            here = (c * half_ep + j == me_e) & (c == core)

            @pl.when(jnp.logical_not(here))
            def _():
                left(rows_out.at[core, pl.ds(0, SLOTS)], sem_r_s.at[j, core])

        return 0

    lax.fori_loop(0, half_ep, sent_back, 0)

    def sent_a(i, _):
        left(att_out.at[pl.ds(0, ht)], sem_a_s.at[i])
        return 0

    lax.fori_loop(1, tp, sent_a, 0)


def default_plan(half_y, shards):
    kv = [("kv", i) for i in range(shards)]
    at = [("attend", i) for i in range(shards)]
    plan = [("slots", 0)]
    plan += [("w", s) for s in range(1, half_y + 1)]
    for a, b in zip(kv, at):
        plan += [a, b]
    plan += [("o_send", 0), ("ffn1", 0), ("ffn2", 0)]
    plan += [("ring", s) for s in range(half_y)]
    plan += [("attend_end", 0), ("ring_end", 0), ("project", 0), ("combine", 0)]
    return plan


def local(g, queries, key_input, value_input, query_gain, key_gain, mix_out_weight, expert_input, ffn_gain,
          routes, route_scores, gate_weight, up_weight, down_weight):
    ep, tp = g.nz * g.nx, g.ny * 2
    kv_at = (lax.axis_index("tp") * g.kv_heads // tp) * HD
    own_k = lax.dynamic_slice_in_dim(key_input, kv_at, HD, 1)
    own_v = lax.dynamic_slice_in_dim(value_input, kv_at, HD, 1)
    kqv = jnp.concatenate([own_k, queries, own_v, own_v], axis=1)
    tables = angle_tables(ep * g.tq // GRID_W)
    half_slots = ep // 2 * SLOTS
    vmem = pl.BlockSpec(memory_space=pltpu.VMEM)
    hbm = pl.BlockSpec(memory_space=pl.ANY)
    yb = g.d // g.ny
    half_y = g.ny // 2
    dma = pltpu.SemaphoreType.DMA
    return pl.pallas_call(
        functools.partial(kernel, g),
        out_shape=(
            jax.ShapeDtypeStruct((g.tq // tp, g.d), BF16),
            jax.ShapeDtypeStruct((g.tok, g.d // tp), BF16),
        ),
        in_specs=[vmem] * 7 + [hbm] + [vmem] * 3 + [hbm] * 4,
        out_specs=(vmem, vmem),
        scratch_shapes=[
            pltpu.VMEM((g.nz, g.tq, 2 * HD), BF16),
            pltpu.VMEM((HD, g.tq), BF16),
            pltpu.VMEM((g.nx, HD, g.tq), BF16),
            pltpu.VMEM((g.nx, 80, g.tq), F32),
            pltpu.VMEM((g.nx, 72, g.tq), F32),
            pltpu.VMEM((g.tq // 2, 2 * HD), BF16),
            pltpu.VMEM((g.tq // 2, 2 * HD), BF16),
            pltpu.VMEM((g.tq, 2 * HD), F32),
            pltpu.VMEM((tp * HD, g.d), BF16),
            pltpu.VMEM((g.tok, g.d // 4), BF16),
            pltpu.VMEM((ep * SLOTS, g.d // 4), BF16),
            pltpu.VMEM((half_slots, g.d), BF16),
            pltpu.VMEM((2, g.d, g.ff), BF16),
            pltpu.VMEM((2, g.d, g.ff), BF16),
            pltpu.VMEM((2 * g.ff, g.d), BF16),
            pltpu.VMEM((2, half_slots, g.ff), F32),
            pltpu.VMEM((2, half_slots, g.ff), F32),
            pltpu.VMEM((half_slots, 128), F32),
            pltpu.VMEM((half_slots, 2 * g.ff), BF16),
            pltpu.VMEM((2, half_y, half_slots, yb), BF16),
            pltpu.VMEM((2, half_y, half_slots, yb), BF16),
            pltpu.VMEM((2, half_slots, yb // 2), BF16),
            pltpu.VMEM((ep * SLOTS, yb // 2), BF16),
            pltpu.VMEM((2, g.tok, ep * SLOTS), BF16),
            dma((5,)),
            dma((g.nz,)), dma((g.nz,)), dma((g.nz,)), dma((g.nz,)),
            dma((g.nx,)), dma((g.nx,)), dma((g.nx,)), dma((g.nx,)),
            dma((tp,)), dma((tp,)),
            dma((2, half_y)), dma((2, half_y)), dma((g.ny,)), dma((g.ny,)),
            dma((3,)), dma((3,)),
            dma((ep,)), dma((ep,)),
            dma((2,)), dma((2,)),
            dma((2, half_y)), dma((2, half_y)),
            dma((ep // 2, 2)), dma((ep,)),
        ],
        compiler_params=pltpu.CompilerParams(
            collective_id=0, has_side_effects=True, vmem_limit_bytes=48 * 1024 * 1024
        ),
    )(
        kqv, key_gain.reshape(1, HD), query_gain.reshape(1, HD), *[jnp.asarray(t) for t in tables],
        expert_input, routes, route_scores, ffn_gain.reshape(1, g.d), mix_out_weight,
        gate_weight, up_weight, down_weight,
    )


SIZES = SimpleNamespace(nz=8, nx=4, ny=8, tq=512, tok=160, d=2048, ff=256, kv_heads=4, plan=default_plan)


def solution(mesh, g=SIZES):
    placed = (
        P("ep", "tp"),
        P("ep", None),
        P("ep", None),
        P(),
        P(),
        P("tp", None),
        P("ep", None),
        P(),
        P("ep", None),
        P("ep", None),
        P("ep", None, "tp"),
        P("ep", None, "tp"),
        P("ep", "tp", None),
    )
    return jax.shard_map(
        functools.partial(local, g),
        mesh=mesh,
        in_specs=placed,
        out_specs=(P(("ep", "tp"), None), P("ep", "tp")),
        check_vma=False,
    )
```

time: 238 us -> 122 us (0.51)
  Pallas kernels: 0 us -> 110 us
  waiting for transfers between devices: 97.3 us -> 0 us
  matrix products: 52.9 us -> 0 us
  blocking collectives: 22.8 us -> 0 us
  local copies, waits for them, and re-layouts: 26 us -> 9.74 us
  between operations: 15.8 us -> 0.78 us
  starting transfers between devices: 14.2 us -> 0 us
  other arithmetic: 6.59 us -> 0.19 us
    pallas_call x0 -> x1, Pallas kernels: none -> 110 us  [local(): pl.pallas_call(functools.partial(kernel, g), out_shape=(jax.ShapeDtypeStr...]
    all_to_all x2 -> x0, waiting for transfers between devices: 55.6 us -> none  [the longest x1 46.3 us: sent_to_all(): return lax.all_to_all(copies, axis, split_axis=0, concat_axis=0, tiled=True)]
    dot_general x35 -> x0, matrix products: 52.9 us -> none  [the longest x16 22.3 us: one_block(): jnp.einsum('qgrd,kgd->qgrk', q_rot, key_block, preferred_element_type=jnp...]
    reduce_scatter x1 -> x0, waiting for transfers between devices: 41.6 us -> none  [local(): lax.psum_scatter(jnp.dot(attended, mix_out_weight, preferred_element_type...]
    all_to_all x1 -> x0, blocking collectives: 22.8 us -> none  [local(): lax.all_to_all(outbound, 'ep', split_axis=0, concat_axis=0, tiled=True)]
    all_to_all x2 -> x0, starting transfers between devices: 13.9 us -> none  [the longest x1 10 us: sent_to_all(): return lax.all_to_all(copies, axis, split_axis=0, concat_axis=0, tiled=True)]
    unnamed x21 -> x33, local copies, waits for them, and re-layouts: 12.5 us -> 8.55 us
    gather x2 -> x0, local copies, waits for them, and re-layouts: 2.92 us -> none  [the longest x1 1.51 us: local(): outbound = padded[owner_row]]
  transfers between devices with their start and end apart: 5 -> 0, of which waited for: 3 -> 0; matrix products, arithmetic and copies ran while one was open for 33% -> 0% of each run, Pallas kernels for 0% -> 0%
where the time goes in v1:
time: 122 us; the launch traced here: 121 us
  Pallas kernels  110 us (90%)
  local copies, waits for them, and re-layouts  9.74 us (8%)
    pallas_call x1, Pallas kernels, local(): pl.pallas_call(functools.partial(kernel, g), out_shape=(jax.ShapeDtypeStr...  110 us
    unnamed x33, local copies, waits for them, and re-layouts  8.55 us

profile of v1, /device:TPU:1, one launch (start us, length us, event | category | flops | bytes accessed | tf_op | source)
XLA Modules:
  0.0 121.1 jit_solution(11203987474242309882)
XLA Ops:
  0.6 0.0 copy-start
  0.7 1.2 constant_dynamic-slice_fusion
  1.9 0.0 copy-start.12
  1.9 1.0 copy.19
  2.8 0.0 copy-start.13
  2.9 0.0 copy-start.4
  2.9 0.0 copy-start.6
  2.9 0.2 pad_maximum_fusion.kqv
  3.1 0.0 copy-done.12
  3.1 0.0 copy-start.5
  3.1 0.1 copy.20.routes
  3.2 0.3 copy-done.13
  3.5 0.0 copy-start.9
  3.5 0.1 copy.21.scores
  3.6 0.0 copy-start.10
  3.7 0.0 copy-start.11
  3.7 0.0 copy-done
  3.7 0.1 copy-done.4
  3.8 0.0 copy-done.6
  3.8 0.2 copy-done.5
  4.0 0.3 copy-done.9
  4.3 0.1 copy-done.10
  4.4 0.0 copy-done.11
  4.4 0.0 copy-start.1
  4.4 1.2 %copy-done.1 = bf16[1,2048,256]{2,1,0:T(8,128)(2,1)S(1)} copy-done((bf16[1,2048,256]{2,1,0:T(8,128)(2,1)S(1)}, bf16[1,2048,256]{2,1,0:T(8,128)(2,1)}, u32[]{:S(2)}) %copy-start.1) | copy-done | bytes 1048600
  5.6 1.2 %copy-done.2 = bf16[1,256,2048]{2,1,0:T(8,128)(2,1)S(1)} copy-done((bf16[1,256,2048]{2,1,0:T(8,128)(2,1)S(1)}, bf16[1,256,2048]{2,1,0:T(8,128)(2,1)}, u32[]{:S(2)}) %copy-start.2) | copy-done | bytes 1048600
  6.8 1.1 copy-done.3
  7.9 0.8 copy-done.7
  8.7 0.8 copy-done.8
  9.4 110.4 %shard_map.176 = (bf16[32,2048]{1,0:T(8,128)(2,1)S(1)}, bf16[160,128]{1,0:T(8,128)(2,1)S(1)}) custom-call(bf16[512,256]{1,0:T(8,128)(2,1)S(1)} %pad_maximum_fusion.kqv, f32[1,64]{1,0:T(1,128)S(1)} %bitcast.4, f32[1,64]{1,0:T(1,128)S(1)} %bitcast.5, f32[256,128]{1,0:T(8,128)S(1)} %copy-done.5, f32[256,128]{1,0:T(8,128)S(1)} %copy-done.6, ...), custom_call_target="tpu_custom_call" | custom-call | tf_op jit(solution)/shard_map/pallas_call | solution.py:668
  119.8 0.7 copy.24
  120.5 0.6 copy.25
  (4 shorter events, 0.0 us)
Async XLA Ops:
  0.6 3.0 %copy-start = (bf16[1,2048,256]{2,1,0:T(8,128)(2,1)S(1)}, bf16[1,2048,256]{2,1,0:T(8,128)(2,1)}, u32[]{:S(2)}) copy-start(bf16[1,2048,256]{2,1,0:T(8,128)(2,1)} %gate_w.1) | copy-start | bytes 3145732
  1.9 1.2 %copy-start.12 = (s32[160,2]{0,1:T(2,128)S(1)}, s32[160,2]{0,1:T(2,128)}, u32[]{:S(2)}) copy-start(s32[160,2]{0,1:T(2,128)} %param.25) | copy-start | bytes 3844
  2.8 0.7 copy-start.13
  2.9 1.0 copy-start.4
  2.9 1.0 copy-start.6
  3.1 0.9 copy-start.5
  3.5 0.7 copy-start.9
  3.6 0.7 copy-start.10
  3.7 0.7 copy-start.11
  4.4 1.2 %copy-start.1 = (bf16[1,2048,256]{2,1,0:T(8,128)(2,1)S(1)}, bf16[1,2048,256]{2,1,0:T(8,128)(2,1)}, u32[]{:S(2)}) copy-start(bf16[1,2048,256]{2,1,0:T(8,128)(2,1)} %up_w.1) | copy-start | bytes 3145732
  5.6 1.2 %copy-start.2 = (bf16[1,256,2048]{2,1,0:T(8,128)(2,1)S(1)}, bf16[1,256,2048]{2,1,0:T(8,128)(2,1)}, u32[]{:S(2)}) copy-start(bf16[1,256,2048]{2,1,0:T(8,128)(2,1)} %down_w.1) | copy-start | bytes 3145732
  6.8 1.1 copy-start.3
  7.9 0.8 copy-start.7
  8.7 0.8 copy-start.8
